TPU v7x, 32 devices: a whole 2x2x4 slice. The times are simulated.
32 devices in a mesh: grp: 2 (over y), fs: 4 (over z), tp: 4 (over x, core).
Axes of the slice: x: 2, y: 2, z: 4, core: 2. Of those that a mesh axis runs over, the one named last changes fastest.
Arguments:
- tokens: bfloat16 [1792, 2048], P(('grp', 'fs'), 'tp'), parts along dimension 0, may hold values from -6 to 6
- route_ids: int32 [1792, 2], P(('grp', 'fs')), parts along dimension 0, may hold values from 0 to 3, all different within a row; in each aligned block of 224 rows (0 to 223, 224 to 447, ...) at most 168 rows name the same one
- route_weights: float32 [1792, 2], P(('grp', 'fs')), parts along dimension 0, may hold values from 0.25 to 1
- norm_gain: float32 [2048], P('fs'), may hold values from 0.1 to 1.9
- gate_master: float32 [4, 2048, 512], P(None, 'fs', 'tp'), may hold values from -0.125 to 0.125
- up_master: float32 [4, 2048, 512], P(None, 'fs', 'tp'), may hold values from -0.125 to 0.125
- down_master: float32 [4, 2048, 512], P(None, 'fs', 'tp'), may hold values from -0.25 to 0.25
Outputs:
- gate_serve: bfloat16 [8, 2048, 512], P(('grp', 'fs'), None, 'tp'), parts along dimension 0
- up_serve: bfloat16 [8, 2048, 512], P(('grp', 'fs'), None, 'tp'), parts along dimension 0
- down_serve: bfloat16 [8, 2048, 512], P(('grp', 'fs'), None, 'tp'), parts along dimension 0
- moe_output: bfloat16 [1792, 2048], P(('grp', 'fs'), 'tp'), parts along dimension 0
There are 2 independent parts, one for each index of `grp`. A program takes and returns all parts, laid end to end along the dimension named above; an argument that names none is the same for every part. Nothing has to cross between parts.
Inputs may be any that keep to these rules, and one draw needn't show every extreme that they name: `route_ids`: the 2 experts of a row differ; within the rows of one index of fs (aligned blocks of 224 rows) no expert is named more than 168 times.
All inputs are finite; a program needn't handle non-finite values.
Results may differ from a plain program's by a relative error of at most 0.012.
Values may be sent and summed in bfloat16 or wider, within the bound.
A program may use at most 64 MiB of HBM per device.

v0:
```python
import jax
import jax.numpy as jnp
from jax import lax
from jax.sharding import PartitionSpec as P

norm_epsilon = 1e-06


def slot_numbers(route_ids, experts, capacity):
    flat_ids = route_ids.reshape(-1)
    onehot = (flat_ids[:, None] == jnp.arange(experts, dtype=jnp.int32)[None, :]).astype(jnp.int32)
    before = jnp.cumsum(onehot, axis=0) - onehot
    position = jnp.sum(before * onehot, axis=1)
    return (flat_ids * capacity + position).reshape(route_ids.shape)


def local(tokens, route_ids, route_weights, norm_gain, gate_master, up_master, down_master):
    experts = gate_master.shape[0]
    shards = lax.axis_size("fs")
    columns = lax.axis_size("tp")
    per_device = experts // shards
    tok_rows = route_ids.shape[0]
    top_count = route_ids.shape[1]
    local_width = tokens.shape[1]
    model_width = local_width * columns
    capacity = max(2, 3 * tok_rows * top_count // (2 * experts))
    row_gain = norm_gain[None, :, None]
    gate_half = (gate_master * row_gain).astype(jnp.bfloat16)
    up_half = (up_master * row_gain).astype(jnp.bfloat16)
    down_half = down_master.astype(jnp.bfloat16)
    gate_serve, up_serve, down_serve = (
        lax.all_to_all(gate_half, "fs", split_axis=0, concat_axis=1, tiled=True),
        lax.all_to_all(up_half, "fs", split_axis=0, concat_axis=1, tiled=True),
        lax.all_to_all(down_half, "fs", split_axis=0, concat_axis=1, tiled=True),
    )
    slot_ids = slot_numbers(route_ids, experts, capacity)
    slot_range = jnp.arange(experts * capacity, dtype=jnp.int32)
    selects = [
        (slot_ids[:, rank_slot, None] == slot_range[None, :]).astype(jnp.bfloat16)
        for rank_slot in range(top_count)
    ]
    placing = selects[0]
    for extra in selects[1:]:
        placing = placing + extra
    local_values = tokens.astype(jnp.float32)
    squares = lax.psum(jnp.sum(local_values * local_values, axis=1), "tp")
    inverse = lax.rsqrt(squares / model_width + norm_epsilon)[:, None]
    normed = (local_values * inverse).astype(jnp.bfloat16)
    buffer = jnp.einsum("ts,td->sd", placing, normed, preferred_element_type=jnp.float32).astype(
        jnp.bfloat16
    )
    arrived = lax.all_to_all(
        buffer.reshape(shards, per_device * capacity, local_width),
        "fs",
        split_axis=0,
        concat_axis=0,
        tiled=True,
    )
    arrived = arrived.reshape(shards, per_device, capacity, local_width)
    partial_value = lax.all_gather(arrived, "tp", axis=3, tiled=True)
    gate_sum = jnp.einsum(
        "sxcd,xdf->xscf", partial_value, gate_serve, preferred_element_type=jnp.float32
    )
    up_sum = jnp.einsum(
        "sxcd,xdf->xscf", partial_value, up_serve, preferred_element_type=jnp.float32
    )
    hidden = (jax.nn.silu(gate_sum) * up_sum).astype(jnp.bfloat16)
    products = jnp.einsum("xdf,xscf->dsxc", down_serve, hidden, preferred_element_type=jnp.float32)
    summed = lax.psum_scatter(
        products.reshape(local_width * lax.axis_size("tp"), shards * per_device * capacity).astype(
            jnp.bfloat16
        ),
        "tp",
        scatter_dimension=0,
        tiled=True,
    )
    returned = lax.all_to_all(
        summed.reshape(local_width, shards, per_device * capacity),
        "fs",
        split_axis=1,
        concat_axis=1,
        tiled=True,
    )
    returned = returned.reshape(local_width, experts * capacity)
    combined = jnp.zeros((tok_rows, local_width), jnp.float32)
    for rank_slot in range(top_count):
        picked = jnp.einsum(
            "ts,ds->td", selects[rank_slot], returned, preferred_element_type=jnp.float32
        )
        combined = combined + route_weights[:, rank_slot : rank_slot + 1] * picked
    return (gate_serve, up_serve, down_serve, combined.astype(jnp.bfloat16))


def solution(mesh):
    placed = (
        P(("grp", "fs"), "tp"),
        P(("grp", "fs"), None),
        P(("grp", "fs"), None),
        P("fs"),
        P(None, "fs", "tp"),
        P(None, "fs", "tp"),
        P(None, "fs", "tp"),
    )
    return jax.shard_map(
        local,
        mesh=mesh,
        in_specs=placed,
        out_specs=(
            P(("grp", "fs"), None, "tp"),
            P(("grp", "fs"), None, "tp"),
            P(("grp", "fs"), None, "tp"),
            P(("grp", "fs"), "tp"),
        ),
        check_vma=False,
    )
```

profile of v0, /device:TPU:0, one launch (start us, length us, event | category | flops | bytes accessed | tf_op | source)
XLA Modules:
  0.0 170.7 jit_solution(8881094231520576288)
XLA Ops:
  7.2 0.0 all-gather.3.cloned.1.call-start
  7.2 0.9 copy.17
  8.2 0.1 eq.52
  8.4 1.2 reduce-window.6
  9.6 0.2 slice_reduce_fusion
  9.8 0.2 reduce-window.9
  10.0 0.1 add_bitcast_fusion
  10.1 0.1 reduce_sum.21
  10.3 0.1 copy.18
  10.3 0.7 multiply_add_fusion
  11.0 1.1 fusion.5
  12.1 8.4 %psum.7 = f32[224]{0:T(256)S(1)} all-reduce(f32[224]{0:T(256)S(1)} %fusion.5), channel_id=1, replica_groups=mesh['grp'=2,'fs'=4,'tp'=4] {'tp'}, use_global_device_ids=true, to_apply=%region_4.5 | all-reduce | flops 224 | bytes 1792 | tf_op jit(solution)/shard_map/psum | solution.py:46
  20.5 1.5 convolution_convert_fusion.1
  22.0 21.6 %all_to_all.46 = bf16[4,168,512]{2,1,0:T(8,128)(2,1)} all-to-all(bf16[4,168,512]{2,1,0:T(8,128)(2,1)S(1)} %bitcast.48), channel_id=1, replica_groups=mesh['grp'=2,'fs'=4,'tp'=4] {'fs'}, dimensions={0} | all-to-all | bytes 1376256 | tf_op jit(solution)/shard_map/all_to_all | solution.py:52
  43.6 1.0 multiply_convert_fusion
  44.6 16.2 %all_to_all.47 = bf16[4,512,128]{2,1,0:T(8,128)(2,1)S(1)} all-to-all(bf16[4,512,128]{2,1,0:T(8,128)(2,1)S(1)} %get-tuple-element.9), channel_id=1, replica_groups=mesh['grp'=2,'fs'=4,'tp'=4] {'fs'}, dimensions={0} | all-to-all | bytes 1048576 | tf_op jit(solution)/shard_map/all_to_all | solution.py:32
  60.9 3.5 %all-to-all-start.1 = ((bf16[4,512,128]{2,1,0:T(8,128)(2,1)}), bf16[4,512,128]{2,1,0:T(8,128)(2,1)S(1)}, u32[]{:S(2)}, u32[]{:S(2)}) async-start(bf16[4,512,128]{2,1,0:T(8,128)(2,1)} %get-tuple-element.8), calls=%async_computation.1 | async-start | bytes 1048576 | tf_op jit(solution)/shard_map/all_to_all | solution.py:33
  64.4 0.9 convert_element_type.49
  65.2 12.6 %all-to-all-done.1 = bf16[4,512,128]{2,1,0:T(8,128)(2,1)S(1)} async-done(((bf16[4,512,128]{2,1,0:T(8,128)(2,1)}), bf16[4,512,128]{2,1,0:T(8,128)(2,1)S(1)}, u32[]{:S(2)}, u32[]{:S(2)}) %all-to-all-start.1) | async-done | bytes 524320 | tf_op jit(solution)/shard_map/all_to_all | solution.py:33
  77.9 4.1 %all-to-all-start.2 = ((bf16[4,512,128]{2,1,0:T(8,128)(2,1)}), bf16[4,512,128]{2,1,0:T(8,128)(2,1)}, u32[]{:S(2)}, u32[]{:S(2)}) async-start(bf16[4,512,128]{2,1,0:T(8,128)(2,1)} %convert_element_type.49), calls=%async_computation.2 | async-start | bytes 1048576 | tf_op jit(solution)/shard_map/all_to_all | solution.py:34
  82.0 0.0 reduce-scatter.2.cloned.1.call-start
  82.1 3.5 %fusion.27 = f32[4,168,128]{2,1,0:T(8,128)} fusion(bf16[4,168,2048]{2,1,0:T(8,128)(2,1)} %all-gather.3.cloned.1.call-done, bf16[2048,128,1]{1,0,2:T(8,128)(2,1)S(1)} %bitcast.41), kind=kOutput, calls=%fused_computation.44 | convolution fusion | flops 352321536 | bytes 3620864 | tf_op jit(solution)/shard_map/sxcd,xdf->xscf/dot_general | solution.py:61
  85.7 10.5 %all-to-all-done.2 = bf16[4,512,128]{2,1,0:T(8,128)(2,1)} async-done(((bf16[4,512,128]{2,1,0:T(8,128)(2,1)}), bf16[4,512,128]{2,1,0:T(8,128)(2,1)}, u32[]{:S(2)}, u32[]{:S(2)}) %all-to-all-start.2) | async-done | bytes 524320 | tf_op jit(solution)/shard_map/all_to_all | solution.py:34
  96.1 5.8 %convolution_convert_fusion = bf16[4,168,2048]{2,1,0:T(8,128)(2,1)} fusion(bf16[2048,128,1]{1,0,2:T(8,128)(2,1)} %bitcast.13, bf16[4,168,2048]{2,1,0:T(8,128)(2,1)S(1)} %copy-done, bf16[2048,128,1]{1,0,2:T(8,128)(2,1)} %bitcast.43, f32[4,168,128]{2,1,0:T(8,128)} %fusion.27), kind=kOutput, calls=%fused_computation | convolution fusion | flops 706535424 | bytes 6897664 | tf_op jit(solution)/shard_map/xdf,xscf->dsxc/dot_general | solution.py:68
  102.0 34.5 %reduce-scatter.2.cloned.1.call-done = bf16[512,672]{0,1:T(8,128)(2,1)} async-done(((bf16[2048,672]{0,1:T(8,128)(2,1)}), bf16[512,672]{0,1:T(8,128)(2,1)}) %reduce-scatter.2.cloned.1.call-update) | async-done | bytes 688144 | tf_op jit(solution)/shard_map/reduce_scatter | solution.py:69
  136.5 4.6 %all-to-all-start.4 = ((bf16[512,4,168]{0,2,1:T(8,128)(2,1)}), bf16[512,4,168]{0,2,1:T(8,128)(2,1)S(1)}, u32[]{:S(2)}, u32[]{:S(2)}) async-start(bf16[512,4,168]{0,2,1:T(8,128)(2,1)} %bitcast.47), calls=%async_computation.5 | async-start | bytes 1376256 | tf_op jit(solution)/shard_map/all_to_all | solution.py:77
  141.1 17.8 %all-to-all-done.4 = bf16[512,4,168]{0,2,1:T(8,128)(2,1)S(1)} async-done(((bf16[512,4,168]{0,2,1:T(8,128)(2,1)}), bf16[512,4,168]{0,2,1:T(8,128)(2,1)S(1)}, u32[]{:S(2)}, u32[]{:S(2)}) %all-to-all-start.4) | async-done | bytes 688160 | tf_op jit(solution)/shard_map/all_to_all | solution.py:77
  158.9 0.4 convolution_multiply_fusion.1
  159.3 1.1 fusion.1
  160.4 0.8 copy.25
  161.2 0.8 copy.26
  162.0 1.9 %copy.27 = bf16[1,2048,128]{2,1,0:T(8,128)(2,1)} copy(bf16[1,2048,128]{2,1,0:T(8,128)(2,1)} %bitcast.2) | data formatting | bytes 1048576
  (27 shorter events, 0.2 us)
Async XLA Ops:
  7.2 36.4 %copy-start.7 = (f32[512]{0:T(512)S(1)}, f32[512]{0:T(512)}, u32[]{:S(2)}) copy-start(f32[512]{0:T(512)} %param.10) | copy-start | bytes 6148
  7.2 36.4 %copy-start.5 = (f32[4,512,128]{2,1,0:T(8,128)S(1)}, f32[4,512,128]{2,1,0:T(8,128)}, u32[]{:S(2)}) copy-start(f32[4,512,128]{2,1,0:T(8,128)} %param.11) | copy-start | bytes 3145732
  7.2 36.4 %copy-start.4 = (f32[4,512,128]{2,1,0:T(8,128)S(1)}, f32[4,512,128]{2,1,0:T(8,128)}, u32[]{:S(2)}) copy-start(f32[4,512,128]{2,1,0:T(8,128)} %param.12) | copy-start | bytes 3145732
  7.2 74.9 %all-gather.3.cloned.1.call-start = ((), (), s32[]{:S(2)}) async-start(), calls=%async_computation.7 | async-start | bytes 3440640 | tf_op jit(solution)/shard_map/all_gather | solution.py:60
  43.6 20.8 %copy-start.3 = (f32[4,512,128]{2,1,0:T(8,128)S(1)}, f32[4,512,128]{2,1,0:T(8,128)}, u32[]{:S(2)}) copy-start(f32[4,512,128]{2,1,0:T(8,128)} %param.13) | copy-start | bytes 3145732
  60.9 17.0 %all-to-all-start.1 = ((bf16[4,512,128]{2,1,0:T(8,128)(2,1)}), bf16[4,512,128]{2,1,0:T(8,128)(2,1)S(1)}, u32[]{:S(2)}, u32[]{:S(2)}) async-start(bf16[4,512,128]{2,1,0:T(8,128)(2,1)} %get-tuple-element.8), calls=%async_computation.1 | async-start | bytes 1048576 | tf_op jit(solution)/shard_map/all_to_all | solution.py:33
  77.9 4.2 %copy-start.1 = (bf16[4,512,128]{2,1,0:T(8,128)(2,1)}, bf16[4,512,128]{2,1,0:T(8,128)(2,1)S(1)}, u32[]{:S(2)}) copy-start(bf16[4,512,128]{2,1,0:T(8,128)(2,1)S(1)} %all-to-all-done.1) | copy-start | bytes 1572868
  77.9 18.3 %all-to-all-start.2 = ((bf16[4,512,128]{2,1,0:T(8,128)(2,1)}), bf16[4,512,128]{2,1,0:T(8,128)(2,1)}, u32[]{:S(2)}, u32[]{:S(2)}) async-start(bf16[4,512,128]{2,1,0:T(8,128)(2,1)} %convert_element_type.49), calls=%async_computation.2 | async-start | bytes 1048576 | tf_op jit(solution)/shard_map/all_to_all | solution.py:34
  82.0 54.5 %reduce-scatter.2.cloned.1.call-start = ((), (), s32[]{:S(2)}) async-start(), calls=%async_computation.6 | async-start | bytes 3440640 | tf_op jit(solution)/shard_map/reduce_scatter | solution.py:69
  82.1 14.0 %copy-start = (bf16[4,168,2048]{2,1,0:T(8,128)(2,1)S(1)}, bf16[4,168,2048]{2,1,0:T(8,128)(2,1)}, u32[]{:S(2)}) copy-start(bf16[4,168,2048]{2,1,0:T(8,128)(2,1)} %all-gather.3.cloned.1.call-done) | copy-start | bytes 8257540
  102.0 39.1 %copy-start.6 = (f32[224,2]{0,1:T(2,128)S(1)}, f32[224,2]{0,1:T(2,128)}, u32[]{:S(2)}) copy-start(f32[224,2]{0,1:T(2,128)} %param.9) | copy-start | bytes 5380
  102.0 59.2 %copy-start.2 = (bf16[4,512,128]{2,1,0:T(8,128)(2,1)S(1)}, bf16[4,512,128]{2,1,0:T(8,128)(2,1)}, u32[]{:S(2)}) copy-start(bf16[4,512,128]{2,1,0:T(8,128)(2,1)} %copy-done.1) | copy-start | bytes 1572868
  136.5 22.4 %all-to-all-start.4 = ((bf16[512,4,168]{0,2,1:T(8,128)(2,1)}), bf16[512,4,168]{0,2,1:T(8,128)(2,1)S(1)}, u32[]{:S(2)}, u32[]{:S(2)}) async-start(bf16[512,4,168]{0,2,1:T(8,128)(2,1)} %bitcast.47), calls=%async_computation.5 | async-start | bytes 1376256 | tf_op jit(solution)/shard_map/all_to_all | solution.py:77
Sparse Core Ops, SparseCore 0:
  43.7 25.4 all-gather.2
  102.1 34.3 reduce-scatter.1
where the time goes:
time: 171 us
  waiting for transfers between devices  75.5 us (44%)
  blocking collectives  46.2 us (27%)
  between operations  14.2 us (8%)
  starting transfers between devices  12.3 us (7%)
  matrix products  12.3 us (7%)
  other arithmetic  5.18 us (3%)
  local copies, waits for them, and re-layouts  5.04 us (3%)
    reduce_scatter x1, waiting for transfers between devices, local(): lax.psum_scatter(products.reshape(local_width * lax.axis_size('tp'), shar...  34.5 us
    all_to_all x1, blocking collectives, local(): lax.all_to_all(buffer.reshape(shards, per_device * capacity, local_width)...  21.6 us
    all_to_all x1, waiting for transfers between devices, local(): lax.all_to_all(summed.reshape(local_width, shards, per_device * capacity)...  17.8 us
    all_to_all x1, blocking collectives, local(): lax.all_to_all(gate_half, 'fs', split_axis=0, concat_axis=1, tiled=True)  16.2 us
    all_to_all x1, waiting for transfers between devices, local(): lax.all_to_all(up_half, 'fs', split_axis=0, concat_axis=1, tiled=True)  12.6 us
    all_to_all x1, waiting for transfers between devices, local(): lax.all_to_all(down_half, 'fs', split_axis=0, concat_axis=1, tiled=True)  10.5 us
    psum x1, blocking collectives, local(): squares = lax.psum(jnp.sum(local_values * local_values, axis=1), 'tp')  8.37 us
    dot_general x1, matrix products, local(): jnp.einsum('xdf,xscf->dsxc', down_serve, hidden, preferred_element_type=j...  5.82 us
  transfers between devices with their start and end apart: 5, of which 4 were waited for; matrix products, arithmetic and copies ran while one was open for 3% of the time, Pallas kernels for 0%

commit v1 on v0

--- a/solution.py
+++ b/solution.py
@@ -1,6 +1,9 @@
+import functools
 import jax
 import jax.numpy as jnp
 from jax import lax
+from jax.experimental import pallas as pl
+from jax.experimental.pallas import tpu as pltpu
 from jax.sharding import PartitionSpec as P
 
 norm_epsilon = 1e-06
@@ -91,7 +94,301 @@
     return (gate_serve, up_serve, down_serve, combined.astype(jnp.bfloat16))
 
 
+MESH = pl.DeviceIdType.MESH
+bf16, f32, i32 = jnp.bfloat16, jnp.float32, jnp.int32
+
+
+def remote(src, dst, send, recv, to):
+    return pltpu.make_async_remote_copy(
+        src_ref=src, dst_ref=dst, send_sem=send, recv_sem=recv, device_id=to, device_id_type=MESH
+    )
+
+
+def kernel(
+    NG, NF, NT, C,
+    tokens, ids, ids_t, weights, gain, gm, um, dm,
+    gate_o, up_o, down_o, moe_o,
+    gmv, umv, dmv, gcol, slots, xs, xg, sd, sgu, wd, wgu, wdq, hid, rs, ret,
+    ld_sem, x_send, x_recv, p_sib, p_x, p_recv,
+    wd_send, wd_recv, wdy_send, wdy_recv, gu_send, gu_recv, guy_send, guy_recv,
+    wq_send, wq_recv, wq_own, h_sib, h_x, h_recv, r_send, r_recv, o_sem,
+):
+    g, f, t = lax.axis_index("grp"), lax.axis_index("fs"), lax.axis_index("tp")
+    NX = NT // 2
+    chip, core = t // 2, lax.rem(t, 2)
+    sib = chip * 2 + (1 - core)
+    H, Fl = dmv.shape[1], dmv.shape[2]
+    Dl = 2 * H
+    T, Dq = tokens.shape
+    E = NF
+    D = NT * Dq
+
+    def fs_at(k):
+        return lax.rem(f + k + NF, NF)
+
+    def rows(s, half):
+        return pl.ds(pl.multiple_of(s * Dl + half * H, H), H)
+
+    halves = [(fs_at(k), g) for k in range(NF)] + [(f, 1 - g)]
+    order = list(range(1, NF)) + [0, NF]
+    loads = {}
+    for m, (src, dst) in ((2, (dm, dmv)), (0, (gm, gmv)), (1, (um, umv))):
+        for k in order:
+            e, half = halves[k]
+            cp = pltpu.make_async_copy(
+                src.at[e, pl.ds(pl.multiple_of(half * H, H), H), :], dst.at[k], ld_sem.at[m, k]
+            )
+            cp.start()
+            loads[m, k] = cp
+
+    barrier = pltpu.get_barrier_semaphore()
+    for k in range(1, NF):
+        pl.semaphore_signal(barrier, inc=1, device_id={"fs": fs_at(k)}, device_id_type=MESH)
+    for k in range(1, NT):
+        pl.semaphore_signal(barrier, inc=1, device_id={"tp": lax.rem(t + k, NT)}, device_id_type=MESH)
+    for k in range(1, NG):
+        pl.semaphore_signal(barrier, inc=1, device_id={"grp": lax.rem(g + k, NG)}, device_id_type=MESH)
+
+    member = jnp.concatenate(
+        [
+            jnp.max((ids_t[...] == e).astype(f32), axis=0, keepdims=True)
+            for e in range(E)
+        ],
+        axis=0,
+    )
+    earlier = (
+        lax.broadcasted_iota(i32, (T, T), 0) < lax.broadcasted_iota(i32, (T, T), 1)
+    ).astype(bf16)
+    pos = jnp.dot(member.astype(bf16), earlier, preferred_element_type=f32)
+    slots[...] = jnp.where(member > 0, pos, -1.0)
+    c_iota = lax.broadcasted_iota(i32, (C, T), 0).astype(f32)
+
+    def placed(e):
+        hot = (c_iota == slots[pl.ds(e, 1), :]).astype(bf16)
+        return jnp.dot(hot, tokens[...], preferred_element_type=f32).astype(bf16)
+
+    for k in range(1, NF):
+        xs[k] = placed(fs_at(k))
+    xg[t, f] = placed(f)
+    pl.semaphore_wait(barrier, (NF - 1) + (NT - 1) + (NG - 1))
+
+    waits = []
+
+    def go(cp):
+        cp.start()
+        waits.append(cp)
+
+    for k in (2, 1, 3, 4, 5, 6, 7):
+        if k < NF:
+            e = fs_at(k)
+            go(remote(xs.at[k], xg.at[t, f], x_send.at[k], x_recv.at[f], {"fs": e}))
+
+    def spread(buf, sems_sib, sems_x, sems_recv, s):
+        go(remote(buf.at[t, s], buf.at[t, s], sems_sib.at[t, s], sems_recv.at[t, s], {"tp": sib}))
+        for dx in range(1, NX):
+            other = lax.rem(chip + dx, NX)
+            go(
+                remote(
+                    buf.at[t, s], buf.at[t, s], sems_x.at[dx, s], sems_recv.at[t, s],
+                    {"tp": other * 2 + core},
+                )
+            )
+
+    def arrived(buf, sems_recv, q, s):
+        remote(buf.at[q, s], buf.at[q, s], sems_recv.at[q, s], sems_recv.at[q, s], {"tp": sib}).wait_recv()
+
+    def pass_on(buf, sems_sib, sems_recv, s):
+        for dx in range(1, NX):
+            q = lax.rem(chip + dx, NX) * 2 + core
+            arrived(buf, sems_recv, q, s)
+            go(remote(buf.at[q, s], buf.at[q, s], sems_sib.at[q, s], sems_recv.at[q, s], {"tp": sib}))
+
+    def sib_arrived(buf, sems_recv, s):
+        for dx in range(NX):
+            arrived(buf, sems_recv, lax.rem(chip + dx, NX) * 2 + 1 - core, s)
+
+    spread(xg, p_sib, p_x, p_recv, f)
+
+    gcol[...] = jnp.transpose(jnp.broadcast_to(gain[...], (Fl, Dl)))
+    for k in range(1, NF):
+        e = fs_at(k)
+        loads[2, k].wait()
+        sd[k] = dmv[k].astype(bf16)
+        go(remote(sd.at[k], wd.at[rows(f, g), :], wd_send.at[k], wd_recv.at[f], {"fs": e}))
+    mine = pl.ds(pl.multiple_of(g * H, H), H)
+    theirs = pl.ds(pl.multiple_of((1 - g) * H, H), H)
+    for k in range(1, NF):
+        e = fs_at(k)
+        loads[0, k].wait()
+        loads[1, k].wait()
+        sgu[k, :, :Fl] = (gmv[k] * gcol[mine, :]).astype(bf16)
+        sgu[k, :, Fl:] = (umv[k] * gcol[mine, :]).astype(bf16)
+        go(remote(sgu.at[k], wgu.at[rows(f, g), :], gu_send.at[k], gu_recv.at[f], {"fs": e}))
+    for k, half, part in ((0, g, mine), (NF, 1 - g, theirs)):
+        for m in range(3):
+            loads[m, k].wait()
+        wd[rows(f, half), :] = dmv[k].astype(bf16)
+        wgu[rows(f, half), :Fl] = (gmv[k] * gcol[part, :]).astype(bf16)
+        wgu[rows(f, half), Fl:] = (umv[k] * gcol[part, :]).astype(bf16)
+
+    near = [k for k in (1, 3, 2, 4, 5, 6, 7) if k < NF]
+    for k in near:
+        s = fs_at(k)
+        remote(xs.at[k], xg.at[t, s], x_send.at[k], x_recv.at[s], {"fs": s}).wait_recv()
+        spread(xg, p_sib, p_x, p_recv, s)
+    pass_on(xg, p_sib, p_recv, f)
+    for k in near:
+        pass_on(xg, p_sib, p_recv, fs_at(k))
+
+    peer = {"grp": lax.rem(g + 1, NG)}
+
+    def to_peer(buf, send, recv, y_send, y_recv, block):
+        for k in near:
+            s = fs_at(k)
+            remote(block.at[k], buf.at[rows(s, g), :], send.at[k], recv.at[s], {"fs": s}).wait_recv()
+            go(remote(buf.at[rows(s, g), :], buf.at[rows(s, g), :], y_send.at[s], y_recv.at[s], peer))
+
+    def from_peer(buf, y_send, y_recv):
+        for k in near:
+            s = fs_at(k)
+            there = buf.at[rows(s, 1 - g), :]
+            remote(there, there, y_send.at[s], y_recv.at[s], peer).wait_recv()
+
+    to_peer(wd, wd_send, wd_recv, wdy_send, wdy_recv, sd)
+    from_peer(wd, wdy_send, wdy_recv)
+
+    def quarter(q):
+        return wd.at[pl.ds(pl.multiple_of(q * Dq, Dq), Dq), :]
+
+    for k in range(1, NT):
+        q = lax.rem(t + k, NT)
+        go(remote(quarter(q), wdq.at[t], wq_send.at[k], wq_recv.at[t], {"tp": q}))
+    own_q = pltpu.make_async_copy(quarter(t), wdq.at[t], wq_own)
+    own_q.start()
+    outs = [pltpu.make_async_copy(wd, down_o.at[0], o_sem.at[2])]
+    outs[0].start()
+
+    for k in range(NF):
+        sib_arrived(xg, p_recv, fs_at(k))
+    to_peer(wgu, gu_send, gu_recv, guy_send, guy_recv, sgu)
+    from_peer(wgu, guy_send, guy_recv)
+    outs.append(pltpu.make_async_copy(wgu.at[:, :Fl], gate_o.at[0], o_sem.at[0]))
+    outs.append(pltpu.make_async_copy(wgu.at[:, Fl:], up_o.at[0], o_sem.at[1]))
+    outs[1].start()
+    outs[2].start()
+
+    far = [k for k in (2, 1, 3, 4, 5, 6, 7) if k < NF] + [0]
+    for k in far:
+        s = fs_at(k)
+        x = jnp.concatenate([xg[q, s] for q in range(NT)], axis=1)
+        xf = x.astype(f32)
+        inv = lax.rsqrt(jnp.sum(xf * xf, axis=1, keepdims=True) / D + norm_epsilon)
+        both = jnp.dot(x, wgu[...], preferred_element_type=f32) * inv
+        gate, up = both[:, :Fl], both[:, Fl:]
+        hid[t, s] = (gate / (1.0 + jnp.exp(-gate)) * up).astype(bf16)
+        spread(hid, h_sib, h_x, h_recv, s)
+    own_q.wait()
+    for k in range(1, NT):
+        q = lax.rem(t + k, NT)
+        remote(wdq.at[q], wdq.at[q], wq_send.at[k], wq_recv.at[q], {"tp": q}).wait_recv()
+    for k in far:
+        pass_on(hid, h_sib, h_recv, fs_at(k))
+    for k in far:
+        s = fs_at(k)
+        sib_arrived(hid, h_recv, s)
+        h = jnp.concatenate([hid[q, s] for q in range(NT)], axis=1)
+        w = jnp.concatenate([wdq[q] for q in range(NT)], axis=1)
+        y = lax.dot_general(h, w, (((1,), (1,)), ((), ())), preferred_element_type=f32).astype(bf16)
+        if k == 0:
+            ret[f] = y
+        else:
+            rs[k] = y
+            go(remote(rs.at[k], ret.at[f], r_send.at[k], r_recv.at[f], {"fs": s}))
+
+    K = ids.shape[1]
+    lane_e = lax.broadcasted_iota(i32, (T, 128), 1)
+    chosen = [ids[:, k : k + 1] for k in range(K)]
+    memb = sum((c == lane_e).astype(f32) for c in chosen)
+    before = (
+        lax.broadcasted_iota(i32, (T, T), 1) < lax.broadcasted_iota(i32, (T, T), 0)
+    ).astype(bf16)
+    place = jnp.dot(before, memb.astype(bf16), preferred_element_type=f32)
+    c_lane = lax.broadcasted_iota(i32, (T, C), 1).astype(f32)
+    total = [jnp.zeros((T, Dq), f32) for _ in range(K)]
+    for k in [0] + near:
+        e = fs_at(k)
+        slot = jnp.sum(jnp.where(lane_e == e, place, 0.0), axis=1, keepdims=True)
+        hits = [(c_lane == jnp.where(c == e, slot, -1.0)).astype(bf16) for c in chosen]
+        if k:
+            remote(rs.at[k], ret.at[e], r_send.at[k], r_recv.at[e], {"fs": e}).wait_recv()
+        block = ret[e]
+        total = [
+            old + jnp.dot(hit, block, preferred_element_type=f32) for old, hit in zip(total, hits)
+        ]
+    out = sum(weights[:, k : k + 1] * total[k] for k in range(K))
+    moe_o[...] = out.astype(bf16)
+    for cp in outs:
+        cp.wait()
+    for cp in waits:
+        cp.wait_send()
+
+
+def fused(tokens, route_ids, route_weights, norm_gain, gate_master, up_master, down_master):
+    NG, NF, NT = (lax.axis_size(a) for a in ("grp", "fs", "tp"))
+    E, Dl, Fl = gate_master.shape
+    T, Dq = tokens.shape
+    capacity = max(2, 3 * T * route_ids.shape[1] // (2 * E))
+    C = -(-capacity // 16) * 16
+    H = Dl // 2
+    D = Dl * NF
+    NX = NT // 2
+    dma = pltpu.SemaphoreType.DMA
+    vmem, hbm = pl.BlockSpec(memory_space=pltpu.VMEM), pl.BlockSpec(memory_space=pl.ANY)
+    serve = jax.ShapeDtypeStruct((1, D, Fl), bf16)
+    return pl.pallas_call(
+        functools.partial(kernel, NG, NF, NT, C),
+        out_shape=(serve, serve, serve, jax.ShapeDtypeStruct((T, Dq), bf16)),
+        in_specs=[vmem] * 5 + [hbm] * 3,
+        out_specs=(hbm, hbm, hbm, vmem),
+        scratch_shapes=[
+            pltpu.VMEM((NF + 1, H, Fl), f32),
+            pltpu.VMEM((NF + 1, H, Fl), f32),
+            pltpu.VMEM((NF + 1, H, Fl), f32),
+            pltpu.VMEM((Dl, Fl), f32),
+            pltpu.VMEM((E, T), f32),
+            pltpu.VMEM((NF, C, Dq), bf16),
+            pltpu.VMEM((NT, NF, C, Dq), bf16),
+            pltpu.VMEM((NF, H, Fl), bf16),
+            pltpu.VMEM((NF, H, 2 * Fl), bf16),
+            pltpu.VMEM((D, Fl), bf16),
+            pltpu.VMEM((D, 2 * Fl), bf16),
+            pltpu.VMEM((NT, Dq, Fl), bf16),
+            pltpu.VMEM((NT, NF, C, Fl), bf16),
+            pltpu.VMEM((NF, C, Dq), bf16),
+            pltpu.VMEM((NF, C, Dq), bf16),
+            dma((3, NF + 1)),
+            dma((NF,)), dma((NF,)),
+            dma((NT, NF)), dma((NX, NF)), dma((NT, NF)),
+            dma((NF,)), dma((NF,)), dma((NF,)), dma((NF,)),
+            dma((NF,)), dma((NF,)), dma((NF,)), dma((NF,)),
+            dma((NT,)), dma((NT,)), dma(()),
+            dma((NT, NF)), dma((NX, NF)), dma((NT, NF)),
+            dma((NF,)), dma((NF,)),
+            dma((3,)),
+        ],
+        compiler_params=pltpu.CompilerParams(
+            collective_id=0, has_side_effects=True, vmem_limit_bytes=56 * 1024 * 1024
+        ),
+    )(
+        tokens, route_ids, route_ids.T, route_weights, norm_gain[None, :],
+        gate_master, up_master, down_master,
+    )
+
+
 def solution(mesh):
+    shape = mesh.shape
+    fits = shape['grp'] == 2 and shape['tp'] % 2 == 0 and shape['fs'] <= 8
+    body = fused if fits else local
     placed = (
         P(("grp", "fs"), "tp"),
         P(("grp", "fs"), None),
@@ -102,7 +399,7 @@
         P(None, "fs", "tp"),
     )
     return jax.shard_map(
-        local,
+        body,
         mesh=mesh,
         in_specs=placed,
         out_specs=(

time: 171 us -> 81.5 us (0.48)
  waiting for transfers between devices: 75.5 us -> 0 us
  Pallas kernels: 0 us -> 73.4 us
  blocking collectives: 46.2 us -> 0 us
  between operations: 14.2 us -> 0.66 us
  matrix products: 12.3 us -> 0 us
  starting transfers between devices: 12.3 us -> 0 us
  other arithmetic: 5.18 us -> 0 us
  local copies, waits for them, and re-layouts: 5.04 us -> 7.22 us
    pallas_call x0 -> x1, Pallas kernels: none -> 73.4 us  [fused(): pl.pallas_call(functools.partial(kernel, NG, NF, NT, C), out_shape=(serve...]
    all_to_all x3 -> x0, waiting for transfers between devices: 40.9 us -> none  [the longest x1 17.8 us: local(): lax.all_to_all(summed.reshape(local_width, shards, per_device * capacity)...]
    all_to_all x2 -> x0, blocking collectives: 37.8 us -> none  [the longest x1 21.6 us: local(): lax.all_to_all(buffer.reshape(shards, per_device * capacity, local_width)...]
    reduce_scatter x1 -> x0, waiting for transfers between devices: 34.5 us -> none  [local(): lax.psum_scatter(products.reshape(local_width * lax.axis_size('tp'), shar...]
    dot_general x5 -> x0, matrix products: 12.3 us -> none  [the longest x1 5.82 us: local(): jnp.einsum('xdf,xscf->dsxc', down_serve, hidden, preferred_element_type=j...]
    all_to_all x3 -> x0, starting transfers between devices: 12.2 us -> none  [the longest x1 4.58 us: local(): lax.all_to_all(summed.reshape(local_width, shards, per_device * capacity)...]
    psum x1 -> x0, blocking collectives: 8.37 us -> none  [local(): squares = lax.psum(jnp.sum(local_values * local_values, axis=1), 'tp')]
    unnamed x21 -> x16, local copies, waits for them, and re-layouts: 4.44 us -> 7.22 us
  transfers between devices with their start and end apart: 5 -> 0, of which waited for: 4 -> 0; matrix products, arithmetic and copies ran while one was open for 3% -> 0% of each run, Pallas kernels for 0% -> 0%
where the time goes in v1:
time: 81.5 us; the launch traced here: 81.2 us
  Pallas kernels  73.4 us (90%)
  local copies, waits for them, and re-layouts  7.22 us (9%)
    pallas_call x1, Pallas kernels, fused(): pl.pallas_call(functools.partial(kernel, NG, NF, NT, C), out_shape=(serve...  73.4 us
    unnamed x16, local copies, waits for them, and re-layouts  7.22 us

profile of v1, /device:TPU:0, one launch (start us, length us, event | category | flops | bytes accessed | tf_op | source)
XLA Modules:
  0.0 81.2 jit_solution(6256912482726579512)
XLA Ops:
  0.6 0.0 copy-start.4
  0.6 0.7 copy-done.4
  1.3 0.0 copy-start.3
  1.3 0.8 copy.12.weights
  2.1 0.0 copy-done.3
  2.1 0.8 copy.11.ids
  2.9 73.4 %shard_map.102 = (bf16[1,2048,128]{2,1,0:T(8,128)(2,1)}, bf16[1,2048,128]{2,1,0:T(8,128)(2,1)}, bf16[1,2048,128]{2,1,0:T(8,128)(2,1)}, bf16[224,512]{1,0:T(8,128)(2,1)}) custom-call(bf16[224,512]{1,0:T(8,128)(2,1)} %tokens.1, s32[224,2]{1,0:T(8,128)} %copy.11.ids, s32[2,224]{1,0:T(2,128)} %bitcast.2, f32[224,2]{1,0:T(8,128)} %copy.12.weights, ...), custom_call_target="tpu_custom_call" | custom-call | tf_op jit(solution)/shard_map/pallas_call | solution.py:348
  76.3 0.0 copy-start.1
  76.3 1.9 %copy.17 = bf16[1,2048,128]{2,1,0:T(8,128)(2,1)} copy(bf16[1,2048,128]{2,1,0:T(8,128)(2,1)} %get-tuple-element.8) | data formatting | bytes 1048576
  78.2 0.0 copy-done.1
  78.2 0.0 copy-start
  78.2 0.8 copy.18
  79.0 0.4 copy-done
  79.4 0.0 copy-start.2
  79.4 0.8 copy.19
  80.2 0.3 copy-done.2
  80.5 0.7 copy.20
Async XLA Ops:
  0.6 0.7 copy-start.4
  1.3 0.8 copy-start.3
  76.3 1.9 %copy-start.1 = (bf16[1,2048,128]{2,1,0:T(8,128)(2,1)S(1)}, bf16[1,2048,128]{2,1,0:T(8,128)(2,1)}, u32[]{:S(2)}) copy-start(bf16[1,2048,128]{2,1,0:T(8,128)(2,1)} %get-tuple-element.9) | copy-start | bytes 1572868
  78.2 1.2 %copy-start = (bf16[1,2048,128]{2,1,0:T(8,128)(2,1)S(1)}, bf16[1,2048,128]{2,1,0:T(8,128)(2,1)}, u32[]{:S(2)}) copy-start(bf16[1,2048,128]{2,1,0:T(8,128)(2,1)} %get-tuple-element.10) | copy-start | bytes 1572868
  79.4 1.1 %copy-start.2 = (bf16[224,512]{1,0:T(8,128)(2,1)S(1)}, bf16[224,512]{1,0:T(8,128)(2,1)}, u32[]{:S(2)}) copy-start(bf16[224,512]{1,0:T(8,128)(2,1)} %get-tuple-element.11) | copy-start | bytes 688132

commit v2 on v1

v2 whole, which is shorter than its diff:
```python
import functools
import jax
import jax.numpy as jnp
from jax import lax
from jax.experimental import pallas as pl
from jax.experimental.pallas import tpu as pltpu
from jax.sharding import PartitionSpec as P

norm_epsilon = 1e-06


def slot_numbers(route_ids, experts, capacity):
    flat_ids = route_ids.reshape(-1)
    onehot = (flat_ids[:, None] == jnp.arange(experts, dtype=jnp.int32)[None, :]).astype(jnp.int32)
    before = jnp.cumsum(onehot, axis=0) - onehot
    position = jnp.sum(before * onehot, axis=1)
    return (flat_ids * capacity + position).reshape(route_ids.shape)


def local(tokens, route_ids, route_weights, norm_gain, gate_master, up_master, down_master):
    experts = gate_master.shape[0]
    shards = lax.axis_size("fs")
    columns = lax.axis_size("tp")
    per_device = experts // shards
    tok_rows = route_ids.shape[0]
    top_count = route_ids.shape[1]
    local_width = tokens.shape[1]
    model_width = local_width * columns
    capacity = max(2, 3 * tok_rows * top_count // (2 * experts))
    row_gain = norm_gain[None, :, None]
    gate_half = (gate_master * row_gain).astype(jnp.bfloat16)
    up_half = (up_master * row_gain).astype(jnp.bfloat16)
    down_half = down_master.astype(jnp.bfloat16)
    gate_serve, up_serve, down_serve = (
        lax.all_to_all(gate_half, "fs", split_axis=0, concat_axis=1, tiled=True),
        lax.all_to_all(up_half, "fs", split_axis=0, concat_axis=1, tiled=True),
        lax.all_to_all(down_half, "fs", split_axis=0, concat_axis=1, tiled=True),
    )
    slot_ids = slot_numbers(route_ids, experts, capacity)
    slot_range = jnp.arange(experts * capacity, dtype=jnp.int32)
    selects = [
        (slot_ids[:, rank_slot, None] == slot_range[None, :]).astype(jnp.bfloat16)
        for rank_slot in range(top_count)
    ]
    placing = selects[0]
    for extra in selects[1:]:
        placing = placing + extra
    local_values = tokens.astype(jnp.float32)
    squares = lax.psum(jnp.sum(local_values * local_values, axis=1), "tp")
    inverse = lax.rsqrt(squares / model_width + norm_epsilon)[:, None]
    normed = (local_values * inverse).astype(jnp.bfloat16)
    buffer = jnp.einsum("ts,td->sd", placing, normed, preferred_element_type=jnp.float32).astype(
        jnp.bfloat16
    )
    arrived = lax.all_to_all(
        buffer.reshape(shards, per_device * capacity, local_width),
        "fs",
        split_axis=0,
        concat_axis=0,
        tiled=True,
    )
    arrived = arrived.reshape(shards, per_device, capacity, local_width)
    partial_value = lax.all_gather(arrived, "tp", axis=3, tiled=True)
    gate_sum = jnp.einsum(
        "sxcd,xdf->xscf", partial_value, gate_serve, preferred_element_type=jnp.float32
    )
    up_sum = jnp.einsum(
        "sxcd,xdf->xscf", partial_value, up_serve, preferred_element_type=jnp.float32
    )
    hidden = (jax.nn.silu(gate_sum) * up_sum).astype(jnp.bfloat16)
    products = jnp.einsum("xdf,xscf->dsxc", down_serve, hidden, preferred_element_type=jnp.float32)
    summed = lax.psum_scatter(
        products.reshape(local_width * lax.axis_size("tp"), shards * per_device * capacity).astype(
            jnp.bfloat16
        ),
        "tp",
        scatter_dimension=0,
        tiled=True,
    )
    returned = lax.all_to_all(
        summed.reshape(local_width, shards, per_device * capacity),
        "fs",
        split_axis=1,
        concat_axis=1,
        tiled=True,
    )
    returned = returned.reshape(local_width, experts * capacity)
    combined = jnp.zeros((tok_rows, local_width), jnp.float32)
    for rank_slot in range(top_count):
        picked = jnp.einsum(
            "ts,ds->td", selects[rank_slot], returned, preferred_element_type=jnp.float32
        )
        combined = combined + route_weights[:, rank_slot : rank_slot + 1] * picked
    return (gate_serve, up_serve, down_serve, combined.astype(jnp.bfloat16))


MESH = pl.DeviceIdType.MESH
bf16, f32, i32 = jnp.bfloat16, jnp.float32, jnp.int32


def remote(src, dst, send, recv, to):
    return pltpu.make_async_remote_copy(
        src_ref=src, dst_ref=dst, send_sem=send, recv_sem=recv, device_id=to, device_id_type=MESH
    )


def kernel(
    NF, NT, C,
    tokens, ids_t, weights_t, gain, gm, um, dm,
    gate_o, up_o, down_o, moe_o,
    gmv, umv, dmv, gcol, toks, ids_all, xg, invs, acc, comb, sd, sgu, wd, wgu, wdq, hid, rs, ret,
    ld_sem, i_send, i_recv, c_send, c_recv, p_sib, p_x, p_recv,
    wd_send, wd_recv, wdy_send, wdy_recv, gu_send, gu_recv, guy_send, guy_recv,
    wq_send, wq_recv, wq_own, h_sib, h_x, h_recv, r_send, r_recv, o_sem,
):
    g, f, t = lax.axis_index("grp"), lax.axis_index("fs"), lax.axis_index("tp")
    NX = NT // 2
    chip, core = t // 2, lax.rem(t, 2)
    sib = chip * 2 + (1 - core)
    H, Fl = dmv.shape[1], dmv.shape[2]
    Dl = 2 * H
    T, Dq = tokens.shape
    D = NT * Dq
    ring = range(1, NF)

    def fs_at(k):
        return lax.rem(f + k + NF, NF)

    def rows(s, half):
        return pl.ds(pl.multiple_of(s * Dl + half * H, H), H)

    def both(s):
        return pl.ds(pl.multiple_of(s * Dl, Dl), Dl)

    halves = [(fs_at(k), g) for k in range(NF)] + [(f, 1 - g)]
    order = list(ring) + [0, NF]
    loads = {}
    for m, src, dst in ((0, gm, gmv), (1, um, umv), (2, dm, dmv)):
        for k in order:
            e, half = halves[k]
            cp = pltpu.make_async_copy(
                src.at[e, pl.ds(pl.multiple_of(half * H, H), H), :], dst.at[k], ld_sem.at[m, k]
            )
            cp.start()
            loads[m, k] = cp

    barrier = pltpu.get_barrier_semaphore()
    for k in ring:
        pl.semaphore_signal(barrier, inc=1, device_id={"fs": fs_at(k)}, device_id_type=MESH)
    for k in range(1, NT):
        pl.semaphore_signal(barrier, inc=1, device_id={"tp": lax.rem(t + k, NT)}, device_id_type=MESH)
    peer = {"grp": 1 - g}
    pl.semaphore_signal(barrier, inc=1, device_id=peer, device_id_type=MESH)

    earlier = (
        lax.broadcasted_iota(i32, (T, T), 0) < lax.broadcasted_iota(i32, (T, T), 1)
    ).astype(bf16)
    c_iota = lax.broadcasted_iota(i32, (C, T), 0).astype(f32)

    def slot_row(ids, e):
        member = jnp.max((ids == e).astype(f32), axis=0, keepdims=True)
        pos = jnp.dot(
            jnp.broadcast_to(member, (8, T)).astype(bf16), earlier, preferred_element_type=f32
        )
        return jnp.where(member > 0, pos[:1], -1.0)

    def place(s, ids, block):
        hot = (c_iota == slot_row(ids, f)).astype(bf16)
        xg[t, s] = jnp.dot(hot, block[...], preferred_element_type=f32).astype(bf16)

    pl.semaphore_wait(barrier, (NF - 1) + (NT - 1) + 1)

    waits = []

    def go(cp):
        cp.start()
        waits.append(cp)

    for k in ring:
        go(remote(ids_t, ids_all.at[f], i_send.at[k], i_recv.at[f], {"fs": fs_at(k)}))

    def hop_right(src, b):
        return remote(src, toks.at[b], c_send.at[0, b], c_recv.at[b], {"fs": f + 1})

    def hop_left(src, b):
        return remote(src, toks.at[b], c_send.at[1, b], c_recv.at[b], {"fs": f - 1})

    @pl.when(f < NF - 1)
    def _():
        hop_right(tokens, f).start()

    @pl.when(f > 0)
    def _():
        hop_left(tokens, f).start()

    def spread(buf, sems_sib, sems_x, sems_recv, s):
        for dx in range(1, NX):
            other = lax.rem(chip + dx, NX)
            remote(
                buf.at[t, s], buf.at[t, s], sems_x.at[dx, s], sems_recv.at[t, s],
                {"tp": other * 2 + core},
            ).start()
        remote(buf.at[t, s], buf.at[t, s], sems_sib.at[t, s], sems_recv.at[t, s], {"tp": sib}).start()

    def arrived(buf, sems_recv, q, s):
        remote(buf.at[q, s], buf.at[q, s], sems_recv.at[q, s], sems_recv.at[q, s], {"tp": sib}).wait_recv()

    def pass_on(buf, sems_sib, sems_recv, s):
        for dx in range(1, NX):
            q = lax.rem(chip + dx, NX) * 2 + core
            arrived(buf, sems_recv, q, s)
            remote(buf.at[q, s], buf.at[q, s], sems_sib.at[q, s], sems_recv.at[q, s], {"tp": sib}).start()

    def sib_arrived(buf, sems_recv, s):
        for dx in range(NX):
            arrived(buf, sems_recv, lax.rem(chip + dx, NX) * 2 + 1 - core, s)

    def spread_sent(buf, sems_sib, sems_x, s):
        for dx in range(1, NX):
            remote(buf.at[t, s], buf.at[t, s], sems_x.at[dx, s], sems_x.at[dx, s], {"tp": sib}).wait_send()
        for dx in range(NX):
            q = lax.rem(chip + dx, NX) * 2 + core
            remote(buf.at[q, s], buf.at[q, s], sems_sib.at[q, s], sems_sib.at[q, s], {"tp": sib}).wait_send()

    place(f, ids_t[...], tokens)
    spread(xg, p_sib, p_x, p_recv, f)

    gcol[...] = jnp.transpose(jnp.broadcast_to(gain[...], (Fl, Dl)))
    mine = pl.ds(pl.multiple_of(g * H, H), H)
    theirs = pl.ds(pl.multiple_of((1 - g) * H, H), H)
    for k in ring:
        loads[0, k].wait()
        loads[1, k].wait()
        sgu[k, :, :Fl] = (gmv[k] * gcol[mine, :]).astype(bf16)
        sgu[k, :, Fl:] = (umv[k] * gcol[mine, :]).astype(bf16)
    for k in ring:
        loads[2, k].wait()
        sd[k] = dmv[k].astype(bf16)

    def gu_copy(k, e):
        return remote(sgu.at[k], wgu.at[rows(f, g), :], gu_send.at[k], gu_recv.at[f], {"fs": e})

    def wd_copy(k, e):
        return remote(sd.at[k], wd.at[rows(f, g), :], wd_send.at[k], wd_recv.at[f], {"fs": e})

    def send_weights(at, way):
        reach = NF - 1 - at if way > 0 else at
        for make in (gu_copy, wd_copy):
            for dist in range(reach, 0, -1):
                make(way * dist % NF, at + way * dist).start()

    def weights_after(d):
        if d < NF - 1:
            @pl.when(f == d)
            def _():
                send_weights(d, 1)

            @pl.when(f == NF - 1 - d)
            def _():
                send_weights(NF - 1 - d, -1)

    weights_after(0)
    for k, half, part in ((0, g, mine), (NF, 1 - g, theirs)):
        for m in range(3):
            loads[m, k].wait()
        wd[rows(f, half), :] = dmv[k].astype(bf16)
        wgu[rows(f, half), :Fl] = (gmv[k] * gcol[part, :]).astype(bf16)
        wgu[rows(f, half), Fl:] = (umv[k] * gcol[part, :]).astype(bf16)

    for k in ring:
        s = fs_at(k)
        remote(ids_t, ids_all.at[s], i_recv.at[s], i_recv.at[s], {"fs": s}).wait_recv()

    def take(b):
        place(b, ids_all[b], toks.at[b])
        spread(xg, p_sib, p_x, p_recv, b)

    for d in ring:
        @pl.when(f >= d)
        def _():
            hop_right(tokens, f - d).wait_recv()

            @pl.when(f < NF - 1)
            def _():
                hop_right(toks.at[f - d], f - d).start()

        @pl.when(f + d < NF)
        def _():
            hop_left(tokens, f + d).wait_recv()

            @pl.when(f > 0)
            def _():
                hop_left(toks.at[f + d], f + d).start()

        weights_after(d)

        @pl.when(f >= d)
        def _():
            take(f - d)

        @pl.when(f + d < NF)
        def _():
            take(f + d)

        if d == 1:
            pass_on(xg, p_sib, p_recv, f)
        else:
            @pl.when(f >= d - 1)
            def _():
                pass_on(xg, p_sib, p_recv, f - d + 1)

            @pl.when(f + d - 1 < NF)
            def _():
                pass_on(xg, p_sib, p_recv, f + d - 1)

    near = [k for k in (1, 3, 2, 4, 5, 6, 7) if k < NF]

    def to_peer(buf, make, y_send, y_recv, recv, k):
        s = fs_at(k)
        here = buf.at[rows(s, g), :]
        remote(here, here, recv.at[s], recv.at[s], {"fs": s}).wait_recv()
        remote(here, here, y_send.at[s], y_recv.at[s], peer).start()

    def from_peer(buf, y_recv, k):
        s = fs_at(k)
        there = buf.at[rows(s, 1 - g), :]
        remote(there, there, y_recv.at[s], y_recv.at[s], peer).wait_recv()

    to_peer(wgu, gu_copy, guy_send, guy_recv, gu_recv, near[0])
    for d in (NF - 1,):
        @pl.when(f >= d)
        def _():
            pass_on(xg, p_sib, p_recv, f - d)

        @pl.when(f + d < NF)
        def _():
            pass_on(xg, p_sib, p_recv, f + d)
    for k in near[1:]:
        to_peer(wgu, gu_copy, guy_send, guy_recv, gu_recv, k)

    for e in range(NF):
        w_row = jnp.sum(jnp.where(ids_t[...] == e, weights_t[...], 0.0), axis=0, keepdims=True)
        w_at = jnp.where(c_iota == slot_row(ids_t[...], e), w_row, 0.0)
        high = w_at.astype(bf16)
        comb[e, :C] = high
        comb[e, C:] = (w_at - high.astype(f32)).astype(bf16)

    for k in range(NF):
        s = fs_at(k)
        sib_arrived(xg, p_recv, s)
        sq = jnp.zeros((C, 1), f32)
        for q in range(NT):
            xf = xg[q, s].astype(f32)
            sq = sq + jnp.sum(xf * xf, axis=1, keepdims=True)
        invs[s] = jnp.broadcast_to(lax.rsqrt(sq / D + norm_epsilon), (C, Fl))

    def partial_sums(s):
        x = xg[s].reshape(NF * C, Dq)
        return jnp.dot(x, wgu[both(s), :], preferred_element_type=f32)

    acc[...] = partial_sums(f)
    for k in near:
        from_peer(wgu, guy_recv, k)
        acc[...] += partial_sums(fs_at(k))
        to_peer(wd, wd_copy, wdy_send, wdy_recv, wd_recv, k)
    outs = [
        pltpu.make_async_copy(wgu.at[:, :Fl], gate_o.at[0], o_sem.at[0]),
        pltpu.make_async_copy(wgu.at[:, Fl:], up_o.at[0], o_sem.at[1]),
        pltpu.make_async_copy(wd, down_o.at[0], o_sem.at[2]),
    ]
    outs[0].start()
    outs[1].start()

    far = [k for k in (2, 1, 3, 4, 5, 6, 7) if k < NF] + [0]
    for k in far:
        s = fs_at(k)
        sums = acc[pl.ds(pl.multiple_of(s * C, 16), C), :]
        gate, up = sums[:, :Fl] * invs[s], sums[:, Fl:] * invs[s]
        hid[t, s] = (gate / (1.0 + jnp.exp(-gate)) * up).astype(bf16)
        spread(hid, h_sib, h_x, h_recv, s)

    def turned(s):
        return remote(wd.at[both(s), :], wdq.at[t], wq_send.at[s], wq_recv.at[t], {"tp": s})

    own_q = pltpu.make_async_copy(wd.at[both(t), :], wdq.at[t], wq_own)
    for k in [0] + near:
        s = fs_at(k)
        if k:
            from_peer(wd, wdy_recv, k)

        @pl.when(s != t)
        def _():
            turned(s).start()

        @pl.when(s == t)
        def _():
            own_q.start()
    outs[2].start()
    for k in far:
        pass_on(hid, h_sib, h_recv, fs_at(k))
    own_q.wait()
    for k in range(1, NT):
        q = lax.rem(t + k, NT)
        remote(wdq.at[q], wdq.at[q], wq_recv.at[q], wq_recv.at[q], {"tp": q}).wait_recv()
    for k in far:
        s = fs_at(k)
        sib_arrived(hid, h_recv, s)
        h = jnp.concatenate([hid[q, s] for q in range(NT)], axis=1)
        w = jnp.concatenate([wdq[q] for q in range(NT)], axis=1)
        y = lax.dot_general(h, w, (((1,), (1,)), ((), ())), preferred_element_type=f32).astype(bf16)
        if k == 0:
            ret[f] = y
        else:
            rs[k] = y
            go(remote(rs.at[k], ret.at[f], r_send.at[k], r_recv.at[f], {"fs": s}))

    total = jnp.zeros((T, Dq), f32)
    for k in [0] + near:
        e = fs_at(k)
        if k:
            remote(rs.at[k], ret.at[e], r_send.at[k], r_recv.at[e], {"fs": e}).wait_recv()
        block = jnp.concatenate([ret[e], ret[e]], axis=0)
        total = total + lax.dot_general(
            comb[e], block, (((0,), (0,)), ((), ())), preferred_element_type=f32
        )
    moe_o[...] = total.astype(bf16)

    for cp in outs:
        cp.wait()
    for cp in waits:
        cp.wait_send()
    for k in ring:
        s = fs_at(k)
        gu_copy(k, s).wait_send()
        wd_copy(k, s).wait_send()
        for buf, y_send in ((wgu, guy_send), (wd, wdy_send)):
            here = buf.at[rows(s, g), :]
            remote(here, here, y_send.at[s], y_send.at[s], peer).wait_send()
    for s in range(NF):
        @pl.when(s != t)
        def _():
            turned(s).wait_send()

        spread_sent(xg, p_sib, p_x, s)
        spread_sent(hid, h_sib, h_x, s)

        @pl.when((s <= f) & (f < NF - 1))
        def _():
            hop_right(tokens, s).wait_send()

        @pl.when((s >= f) & (f > 0))
        def _():
            hop_left(tokens, s).wait_send()


def fused(tokens, route_ids, route_weights, norm_gain, gate_master, up_master, down_master):
    NF, NT = lax.axis_size("fs"), lax.axis_size("tp")
    E, Dl, Fl = gate_master.shape
    T, Dq = tokens.shape
    K = route_ids.shape[1]
    capacity = max(2, 3 * T * K // (2 * E))
    C = -(-capacity // 16) * 16
    H = Dl // 2
    D = Dl * NF
    NX = NT // 2
    dma = pltpu.SemaphoreType.DMA
    vmem, hbm = pl.BlockSpec(memory_space=pltpu.VMEM), pl.BlockSpec(memory_space=pl.ANY)
    serve = jax.ShapeDtypeStruct((1, D, Fl), bf16)
    return pl.pallas_call(
        functools.partial(kernel, NF, NT, C),
        out_shape=(serve, serve, serve, jax.ShapeDtypeStruct((T, Dq), bf16)),
        in_specs=[vmem] * 4 + [hbm] * 3,
        out_specs=(hbm, hbm, hbm, vmem),
        scratch_shapes=[
            pltpu.VMEM((NF + 1, H, Fl), f32),
            pltpu.VMEM((NF + 1, H, Fl), f32),
            pltpu.VMEM((NF + 1, H, Fl), f32),
            pltpu.VMEM((Dl, Fl), f32),
            pltpu.VMEM((NF, T, Dq), bf16),
            pltpu.VMEM((NF, K, T), i32),
            pltpu.VMEM((NT, NF, C, Dq), bf16),
            pltpu.VMEM((NF, C, Fl), f32),
            pltpu.VMEM((NF * C, 2 * Fl), f32),
            pltpu.VMEM((NF, 2 * C, T), bf16),
            pltpu.VMEM((NF, H, Fl), bf16),
            pltpu.VMEM((NF, H, 2 * Fl), bf16),
            pltpu.VMEM((D, Fl), bf16),
            pltpu.VMEM((D, 2 * Fl), bf16),
            pltpu.VMEM((NT, Dq, Fl), bf16),
            pltpu.VMEM((NT, NF, C, Fl), bf16),
            pltpu.VMEM((NF, C, Dq), bf16),
            pltpu.VMEM((NF, C, Dq), bf16),
            dma((3, NF + 1)),
            dma((NF,)), dma((NF,)),
            dma((2, NF)), dma((NF,)),
            dma((NT, NF)), dma((NX, NF)), dma((NT, NF)),
            dma((NF,)), dma((NF,)), dma((NF,)), dma((NF,)),
            dma((NF,)), dma((NF,)), dma((NF,)), dma((NF,)),
            dma((NT,)), dma((NT,)), dma(()),
            dma((NT, NF)), dma((NX, NF)), dma((NT, NF)),
            dma((NF,)), dma((NF,)),
            dma((3,)),
        ],
        compiler_params=pltpu.CompilerParams(
            collective_id=0, has_side_effects=True, vmem_limit_bytes=56 * 1024 * 1024
        ),
    )(
        tokens, route_ids.T, route_weights.T, norm_gain[None, :],
        gate_master, up_master, down_master,
    )


def solution(mesh):
    shape = mesh.shape
    fits = shape['grp'] == 2 and shape['tp'] % 2 == 0 and shape['fs'] == shape['tp'] <= 8
    body = fused if fits else local
    placed = (
        P(("grp", "fs"), "tp"),
        P(("grp", "fs"), None),
        P(("grp", "fs"), None),
        P("fs"),
        P(None, "fs", "tp"),
        P(None, "fs", "tp"),
        P(None, "fs", "tp"),
    )
    return jax.shard_map(
        body,
        mesh=mesh,
        in_specs=placed,
        out_specs=(
            P(("grp", "fs"), None, "tp"),
            P(("grp", "fs"), None, "tp"),
            P(("grp", "fs"), None, "tp"),
            P(("grp", "fs"), "tp"),
        ),
        check_vma=False,
    )
```

time: 81.5 us -> 80.6 us (0.989); the launches traced: 81.2 us -> 79.1 us
  local copies, waits for them, and re-layouts: 7.22 us -> 4.97 us
    unnamed x16 -> x10, local copies, waits for them, and re-layouts: 7.22 us -> 4.97 us
where the time goes in v2:
time: 80.6 us; the launch traced here: 79.1 us
  Pallas kernels  73.4 us (91%)
  local copies, waits for them, and re-layouts  4.97 us (6%)
    pallas_call x1, Pallas kernels, fused(): pl.pallas_call(functools.partial(kernel, NF, NT, C), out_shape=(serve, se...  73.4 us
    unnamed x10, local copies, waits for them, and re-layouts  4.97 us

profile of v2, /device:TPU:0, one launch (start us, length us, event | category | flops | bytes accessed | tf_op | source)
XLA Modules:
  0.0 79.1 jit_solution(11974164406421284984)
XLA Ops:
  0.6 73.4 %shard_map.102 = (bf16[1,2048,128]{2,1,0:T(8,128)(2,1)}, bf16[1,2048,128]{2,1,0:T(8,128)(2,1)}, bf16[1,2048,128]{2,1,0:T(8,128)(2,1)}, bf16[224,512]{1,0:T(8,128)(2,1)}) custom-call(bf16[224,512]{1,0:T(8,128)(2,1)} %tokens.1, s32[2,224]{1,0:T(2,128)} %bitcast.3, f32[2,224]{1,0:T(2,128)} %bitcast.4, f32[1,512]{1,0:T(1,128)} %bitcast.5, f32[4,512,128]{2,1,0:T(8,128)} %gm.1, ...), custom_call_target="tpu_custom_call" | custom-call | tf_op jit(solution)/shard_map/pallas_call | solution.py:469
  74.1 0.0 copy-start.1
  74.1 1.9 %copy.15 = bf16[1,2048,128]{2,1,0:T(8,128)(2,1)} copy(bf16[1,2048,128]{2,1,0:T(8,128)(2,1)} %get-tuple-element.8) | data formatting | bytes 1048576
  76.0 0.0 copy-done.1
  76.0 0.0 copy-start
  76.0 0.8 %copy.16 = bf16[1,2048,128]{2,1,0:T(8,128)(2,1)} copy(bf16[1,2048,128]{2,1,0:T(8,128)(2,1)S(1)} %copy-done.1) | data formatting | bytes 1048576
  76.8 0.4 copy-done
  77.2 0.0 copy-start.2
  77.2 0.8 %copy.17 = bf16[1,2048,128]{2,1,0:T(8,128)(2,1)} copy(bf16[1,2048,128]{2,1,0:T(8,128)(2,1)S(1)} %copy-done) | data formatting | bytes 1048576
  78.0 0.3 copy-done.2
  78.4 0.7 copy.18
Async XLA Ops:
  74.1 1.9 %copy-start.1 = (bf16[1,2048,128]{2,1,0:T(8,128)(2,1)S(1)}, bf16[1,2048,128]{2,1,0:T(8,128)(2,1)}, u32[]{:S(2)}) copy-start(bf16[1,2048,128]{2,1,0:T(8,128)(2,1)} %get-tuple-element.9) | copy-start | bytes 1572868
  76.0 1.2 %copy-start = (bf16[1,2048,128]{2,1,0:T(8,128)(2,1)S(1)}, bf16[1,2048,128]{2,1,0:T(8,128)(2,1)}, u32[]{:S(2)}) copy-start(bf16[1,2048,128]{2,1,0:T(8,128)(2,1)} %get-tuple-element.10) | copy-start | bytes 1572868
  77.2 1.1 %copy-start.2 = (bf16[224,512]{1,0:T(8,128)(2,1)S(1)}, bf16[224,512]{1,0:T(8,128)(2,1)}, u32[]{:S(2)}) copy-start(bf16[224,512]{1,0:T(8,128)(2,1)} %get-tuple-element.11) | copy-start | bytes 688132

commit v3 on v2

--- a/solution.py
+++ b/solution.py
@@ -245,9 +245,13 @@
 
     def send_weights(at, way):
         reach = NF - 1 - at if way > 0 else at
-        for make in (gu_copy, wd_copy):
-            for dist in range(reach, 0, -1):
-                make(way * dist % NF, at + way * dist).start()
+        jobs = [(gu_copy, dist) for dist in range(1, reach + 1)]
+        jobs += [(wd_copy, dist) for dist in range(1, reach + 1)]
+        if reach == NF - 1:
+            jobs.remove((wd_copy, 1))
+            jobs.insert(1, (wd_copy, 1))
+        for make, dist in jobs:
+            make(way * dist % NF, at + way * dist).start()
 
     def weights_after(d):
         if d < NF - 1:
@@ -313,20 +317,26 @@
             def _():
                 pass_on(xg, p_sib, p_recv, f + d - 1)
 
-    near = [k for k in (1, 3, 2, 4, 5, 6, 7) if k < NF]
-
-    def to_peer(buf, make, y_send, y_recv, recv, k):
-        s = fs_at(k)
+    by_distance = [sorted((s for s in range(NF) if s != a), key=lambda s: abs(s - a)) for a in range(NF)]
+
+    def pick(column):
+        out = jnp.int32(column[0])
+        for a in range(1, NF):
+            out = jnp.where(f == a, jnp.int32(column[a]), out)
+        return out
+
+    near = [pick([by_distance[a][i] for a in range(NF)]) for i in range(NF - 1)]
+
+    def to_peer(buf, y_send, y_recv, recv, s):
         here = buf.at[rows(s, g), :]
         remote(here, here, recv.at[s], recv.at[s], {"fs": s}).wait_recv()
         remote(here, here, y_send.at[s], y_recv.at[s], peer).start()
 
-    def from_peer(buf, y_recv, k):
-        s = fs_at(k)
+    def from_peer(buf, y_recv, s):
         there = buf.at[rows(s, 1 - g), :]
         remote(there, there, y_recv.at[s], y_recv.at[s], peer).wait_recv()
 
-    to_peer(wgu, gu_copy, guy_send, guy_recv, gu_recv, near[0])
+    to_peer(wgu, guy_send, guy_recv, gu_recv, near[0])
     for d in (NF - 1,):
         @pl.when(f >= d)
         def _():
@@ -335,15 +345,15 @@
         @pl.when(f + d < NF)
         def _():
             pass_on(xg, p_sib, p_recv, f + d)
-    for k in near[1:]:
-        to_peer(wgu, gu_copy, guy_send, guy_recv, gu_recv, k)
+    for s in near[1:]:
+        to_peer(wgu, guy_send, guy_recv, gu_recv, s)
 
     for e in range(NF):
         w_row = jnp.sum(jnp.where(ids_t[...] == e, weights_t[...], 0.0), axis=0, keepdims=True)
         w_at = jnp.where(c_iota == slot_row(ids_t[...], e), w_row, 0.0)
         high = w_at.astype(bf16)
-        comb[e, :C] = high
-        comb[e, C:] = (w_at - high.astype(f32)).astype(bf16)
+        comb[e, 0] = high
+        comb[e, 1] = (w_at - high.astype(f32)).astype(bf16)
 
     for k in range(NF):
         s = fs_at(k)
@@ -354,15 +364,33 @@
             sq = sq + jnp.sum(xf * xf, axis=1, keepdims=True)
         invs[s] = jnp.broadcast_to(lax.rsqrt(sq / D + norm_epsilon), (C, Fl))
 
-    def partial_sums(s):
-        x = xg[s].reshape(NF * C, Dq)
-        return jnp.dot(x, wgu[both(s), :], preferred_element_type=f32)
-
-    acc[...] = partial_sums(f)
-    for k in near:
-        from_peer(wgu, guy_recv, k)
-        acc[...] += partial_sums(fs_at(k))
-        to_peer(wd, wd_copy, wdy_send, wdy_recv, wd_recv, k)
+    def partial_sums(q, first):
+        w = wgu[both(q), :]
+        for s in range(NF):
+            part = jnp.dot(xg[q, s], w, preferred_element_type=f32)
+            acc[s] = part if first else acc[s] + part
+
+    def turned(s, half):
+        part = pl.ds(pl.multiple_of(half * H, H), H)
+        return remote(
+            wd.at[rows(s, half), :], wdq.at[t, part, :], wq_send.at[s, half], wq_recv.at[t, half], {"tp": s}
+        )
+
+    own_q = pltpu.make_async_copy(wd.at[both(t), :], wdq.at[t], wq_own)
+
+    def turn(s, half):
+        @pl.when(s != t)
+        def _():
+            turned(s, half).start()
+
+    turn(f, 0)
+    turn(f, 1)
+    partial_sums(f, True)
+    for s in near:
+        from_peer(wgu, guy_recv, s)
+        partial_sums(s, False)
+        to_peer(wd, wdy_send, wdy_recv, wd_recv, s)
+        turn(s, g)
     outs = [
         pltpu.make_async_copy(wgu.at[:, :Fl], gate_o.at[0], o_sem.at[0]),
         pltpu.make_async_copy(wgu.at[:, Fl:], up_o.at[0], o_sem.at[1]),
@@ -371,58 +399,45 @@
     outs[0].start()
     outs[1].start()
 
-    far = [k for k in (2, 1, 3, 4, 5, 6, 7) if k < NF] + [0]
-    for k in far:
-        s = fs_at(k)
-        sums = acc[pl.ds(pl.multiple_of(s * C, 16), C), :]
+    far = near[::-1] + [f]
+    for s in far:
+        sums = acc[s]
         gate, up = sums[:, :Fl] * invs[s], sums[:, Fl:] * invs[s]
         hid[t, s] = (gate / (1.0 + jnp.exp(-gate)) * up).astype(bf16)
         spread(hid, h_sib, h_x, h_recv, s)
 
-    def turned(s):
-        return remote(wd.at[both(s), :], wdq.at[t], wq_send.at[s], wq_recv.at[t], {"tp": s})
-
-    own_q = pltpu.make_async_copy(wd.at[both(t), :], wdq.at[t], wq_own)
-    for k in [0] + near:
-        s = fs_at(k)
-        if k:
-            from_peer(wd, wdy_recv, k)
-
-        @pl.when(s != t)
-        def _():
-            turned(s).start()
-
-        @pl.when(s == t)
-        def _():
-            own_q.start()
+    for s in near:
+        from_peer(wd, wdy_recv, s)
+        turn(s, 1 - g)
+    own_q.start()
     outs[2].start()
-    for k in far:
-        pass_on(hid, h_sib, h_recv, fs_at(k))
+    for s in far:
+        pass_on(hid, h_sib, h_recv, s)
     own_q.wait()
     for k in range(1, NT):
         q = lax.rem(t + k, NT)
-        remote(wdq.at[q], wdq.at[q], wq_recv.at[q], wq_recv.at[q], {"tp": q}).wait_recv()
-    for k in far:
-        s = fs_at(k)
+        for half in range(2):
+            part = wdq.at[q, half * H : (half + 1) * H, :]
+            remote(part, part, wq_recv.at[q, half], wq_recv.at[q, half], {"tp": q}).wait_recv()
+    for i, s in enumerate(far):
         sib_arrived(hid, h_recv, s)
         h = jnp.concatenate([hid[q, s] for q in range(NT)], axis=1)
         w = jnp.concatenate([wdq[q] for q in range(NT)], axis=1)
         y = lax.dot_general(h, w, (((1,), (1,)), ((), ())), preferred_element_type=f32).astype(bf16)
-        if k == 0:
+        if i == NF - 1:
             ret[f] = y
         else:
-            rs[k] = y
-            go(remote(rs.at[k], ret.at[f], r_send.at[k], r_recv.at[f], {"fs": s}))
+            rs[s] = y
+            go(remote(rs.at[s], ret.at[f], r_send.at[s], r_recv.at[f], {"fs": s}))
 
     total = jnp.zeros((T, Dq), f32)
-    for k in [0] + near:
-        e = fs_at(k)
-        if k:
-            remote(rs.at[k], ret.at[e], r_send.at[k], r_recv.at[e], {"fs": e}).wait_recv()
-        block = jnp.concatenate([ret[e], ret[e]], axis=0)
-        total = total + lax.dot_general(
-            comb[e], block, (((0,), (0,)), ((), ())), preferred_element_type=f32
-        )
+    for i, e in enumerate([f] + near):
+        if i:
+            remote(rs.at[e], ret.at[e], r_recv.at[e], r_recv.at[e], {"fs": e}).wait_recv()
+        for term in range(2):
+            total = total + lax.dot_general(
+                comb[e, term], ret[e], (((0,), (0,)), ((), ())), preferred_element_type=f32
+            )
     moe_o[...] = total.astype(bf16)
 
     for cp in outs:
@@ -439,7 +454,8 @@
     for s in range(NF):
         @pl.when(s != t)
         def _():
-            turned(s).wait_send()
+            turned(s, 0).wait_send()
+            turned(s, 1).wait_send()
 
         spread_sent(xg, p_sib, p_x, s)
         spread_sent(hid, h_sib, h_x, s)
@@ -459,7 +475,7 @@
     T, Dq = tokens.shape
     K = route_ids.shape[1]
     capacity = max(2, 3 * T * K // (2 * E))
-    C = -(-capacity // 16) * 16
+    C = -(-capacity // 8) * 8
     H = Dl // 2
     D = Dl * NF
     NX = NT // 2
@@ -480,8 +496,8 @@
             pltpu.VMEM((NF, K, T), i32),
             pltpu.VMEM((NT, NF, C, Dq), bf16),
             pltpu.VMEM((NF, C, Fl), f32),
-            pltpu.VMEM((NF * C, 2 * Fl), f32),
-            pltpu.VMEM((NF, 2 * C, T), bf16),
+            pltpu.VMEM((NF, C, 2 * Fl), f32),
+            pltpu.VMEM((NF, 2, C, T), bf16),
             pltpu.VMEM((NF, H, Fl), bf16),
             pltpu.VMEM((NF, H, 2 * Fl), bf16),
             pltpu.VMEM((D, Fl), bf16),
@@ -496,7 +512,7 @@
             dma((NT, NF)), dma((NX, NF)), dma((NT, NF)),
             dma((NF,)), dma((NF,)), dma((NF,)), dma((NF,)),
             dma((NF,)), dma((NF,)), dma((NF,)), dma((NF,)),
-            dma((NT,)), dma((NT,)), dma(()),
+            dma((NT, 2)), dma((NT, 2)), dma(()),
             dma((NT, NF)), dma((NX, NF)), dma((NT, NF)),
             dma((NF,)), dma((NF,)),
             dma((3,)),

time: 80.6 us -> 76 us (0.943)
  the two profiles are of different devices: /device:TPU:0 before, /device:TPU:11 now
where the time goes in v3:
time: 76 us; the launch traced here: 75.7 us
  Pallas kernels  70.1 us (92%)
  local copies, waits for them, and re-layouts  4.97 us (7%)
    pallas_call x1, Pallas kernels, fused(): pl.pallas_call(functools.partial(kernel, NF, NT, C), out_shape=(serve, se...  70.1 us
    unnamed x10, local copies, waits for them, and re-layouts  4.97 us

profile of v3, /device:TPU:11, one launch (start us, length us, event | category | flops | bytes accessed | tf_op | source)
XLA Modules:
  0.0 75.7 jit_solution(79645694810887623)
XLA Ops:
  0.6 70.1 %shard_map.102 = (bf16[1,2048,128]{2,1,0:T(8,128)(2,1)}, bf16[1,2048,128]{2,1,0:T(8,128)(2,1)}, bf16[1,2048,128]{2,1,0:T(8,128)(2,1)}, bf16[224,512]{1,0:T(8,128)(2,1)}) custom-call(bf16[224,512]{1,0:T(8,128)(2,1)} %tokens.1, s32[2,224]{1,0:T(2,128)} %bitcast.3, f32[2,224]{1,0:T(2,128)} %bitcast.4, f32[1,512]{1,0:T(1,128)} %bitcast.5, f32[4,512,128]{2,1,0:T(8,128)} %gm.1, ...), custom_call_target="tpu_custom_call" | custom-call | tf_op jit(solution)/shard_map/pallas_call | solution.py:485
  70.7 0.0 copy-start.1
  70.7 1.9 %copy.15 = bf16[1,2048,128]{2,1,0:T(8,128)(2,1)} copy(bf16[1,2048,128]{2,1,0:T(8,128)(2,1)} %get-tuple-element.8) | data formatting | bytes 1048576
  72.7 0.0 copy-done.1
  72.7 0.0 copy-start
  72.7 0.8 %copy.16 = bf16[1,2048,128]{2,1,0:T(8,128)(2,1)} copy(bf16[1,2048,128]{2,1,0:T(8,128)(2,1)S(1)} %copy-done.1) | data formatting | bytes 1048576
  73.5 0.4 copy-done
  73.9 0.0 copy-start.2
  73.9 0.8 %copy.17 = bf16[1,2048,128]{2,1,0:T(8,128)(2,1)} copy(bf16[1,2048,128]{2,1,0:T(8,128)(2,1)S(1)} %copy-done) | data formatting | bytes 1048576
  74.7 0.3 copy-done.2
  75.0 0.7 copy.18
Async XLA Ops:
  70.7 1.9 %copy-start.1 = (bf16[1,2048,128]{2,1,0:T(8,128)(2,1)S(1)}, bf16[1,2048,128]{2,1,0:T(8,128)(2,1)}, u32[]{:S(2)}) copy-start(bf16[1,2048,128]{2,1,0:T(8,128)(2,1)} %get-tuple-element.9) | copy-start | bytes 1572868
  72.7 1.2 %copy-start = (bf16[1,2048,128]{2,1,0:T(8,128)(2,1)S(1)}, bf16[1,2048,128]{2,1,0:T(8,128)(2,1)}, u32[]{:S(2)}) copy-start(bf16[1,2048,128]{2,1,0:T(8,128)(2,1)} %get-tuple-element.10) | copy-start | bytes 1572868
  73.9 1.1 %copy-start.2 = (bf16[224,512]{1,0:T(8,128)(2,1)S(1)}, bf16[224,512]{1,0:T(8,128)(2,1)}, u32[]{:S(2)}) copy-start(bf16[224,512]{1,0:T(8,128)(2,1)} %get-tuple-element.11) | copy-start | bytes 688132

commit v4 on v3

--- a/solution.py
+++ b/solution.py
@@ -179,19 +179,24 @@
     for k in ring:
         go(remote(ids_t, ids_all.at[f], i_send.at[k], i_recv.at[f], {"fs": fs_at(k)}))
 
-    def hop_right(src, b):
-        return remote(src, toks.at[b], c_send.at[0, b], c_recv.at[b], {"fs": f + 1})
-
-    def hop_left(src, b):
-        return remote(src, toks.at[b], c_send.at[1, b], c_recv.at[b], {"fs": f - 1})
+    parts = 2 if T % 32 == 0 else 1
+    Tp = T // parts
+
+    def hop(src, b, p, way):
+        cut = pl.ds(p * Tp, Tp)
+        return remote(
+            src.at[cut, :], toks.at[b, cut, :], c_send.at[(1 - way) // 2, b, p], c_recv.at[b, p], {"fs": f + way}
+        )
 
     @pl.when(f < NF - 1)
     def _():
-        hop_right(tokens, f).start()
+        for p in range(parts):
+            hop(tokens, f, p, 1).start()
 
     @pl.when(f > 0)
     def _():
-        hop_left(tokens, f).start()
+        for p in range(parts):
+            hop(tokens, f, p, -1).start()
 
     def spread(buf, sems_sib, sems_x, sems_recv, s):
         for dx in range(1, NX):
@@ -245,25 +250,10 @@
 
     def send_weights(at, way):
         reach = NF - 1 - at if way > 0 else at
-        jobs = [(gu_copy, dist) for dist in range(1, reach + 1)]
-        jobs += [(wd_copy, dist) for dist in range(1, reach + 1)]
-        if reach == NF - 1:
-            jobs.remove((wd_copy, 1))
-            jobs.insert(1, (wd_copy, 1))
-        for make, dist in jobs:
-            make(way * dist % NF, at + way * dist).start()
-
-    def weights_after(d):
-        if d < NF - 1:
-            @pl.when(f == d)
-            def _():
-                send_weights(d, 1)
-
-            @pl.when(f == NF - 1 - d)
-            def _():
-                send_weights(NF - 1 - d, -1)
-
-    weights_after(0)
+        for make in (gu_copy, wd_copy):
+            for dist in range(1, reach + 1):
+                make(way * dist % NF, at + way * dist).start()
+
     for k, half, part in ((0, g, mine), (NF, 1 - g, theirs)):
         for m in range(3):
             loads[m, k].wait()
@@ -280,23 +270,29 @@
         spread(xg, p_sib, p_x, p_recv, b)
 
     for d in ring:
-        @pl.when(f >= d)
-        def _():
-            hop_right(tokens, f - d).wait_recv()
-
-            @pl.when(f < NF - 1)
+        for p in range(parts):
+            @pl.when(f >= d)
             def _():
-                hop_right(toks.at[f - d], f - d).start()
-
-        @pl.when(f + d < NF)
-        def _():
-            hop_left(tokens, f + d).wait_recv()
-
-            @pl.when(f > 0)
+                hop(tokens, f - d, p, 1).wait_recv()
+
+                @pl.when(f < NF - 1)
+                def _():
+                    hop(toks.at[f - d], f - d, p, 1).start()
+
+            @pl.when(f + d < NF)
             def _():
-                hop_left(toks.at[f + d], f + d).start()
-
-        weights_after(d)
+                hop(tokens, f + d, p, -1).wait_recv()
+
+                @pl.when(f > 0)
+                def _():
+                    hop(toks.at[f + d], f + d, p, -1).start()
+
+        for at in range(NF):
+            if max(at, NF - 1 - at) == d:
+                @pl.when(f == at)
+                def _():
+                    send_weights(at, 1)
+                    send_weights(at, -1)
 
         @pl.when(f >= d)
         def _():
@@ -460,13 +456,14 @@
         spread_sent(xg, p_sib, p_x, s)
         spread_sent(hid, h_sib, h_x, s)
 
-        @pl.when((s <= f) & (f < NF - 1))
-        def _():
-            hop_right(tokens, s).wait_send()
-
-        @pl.when((s >= f) & (f > 0))
-        def _():
-            hop_left(tokens, s).wait_send()
+        for p in range(parts):
+            @pl.when((s <= f) & (f < NF - 1))
+            def _():
+                hop(tokens, s, p, 1).wait_send()
+
+            @pl.when((s >= f) & (f > 0))
+            def _():
+                hop(tokens, s, p, -1).wait_send()
 
 
 def fused(tokens, route_ids, route_weights, norm_gain, gate_master, up_master, down_master):
@@ -508,7 +505,7 @@
             pltpu.VMEM((NF, C, Dq), bf16),
             dma((3, NF + 1)),
             dma((NF,)), dma((NF,)),
-            dma((2, NF)), dma((NF,)),
+            dma((2, NF, 2)), dma((NF, 2)),
             dma((NT, NF)), dma((NX, NF)), dma((NT, NF)),
             dma((NF,)), dma((NF,)), dma((NF,)), dma((NF,)),
             dma((NF,)), dma((NF,)), dma((NF,)), dma((NF,)),

time: 76 us -> 69 us (0.908)
  the two profiles are of different devices: /device:TPU:11 before, /device:TPU:0 now
where the time goes in v4:
time: 69 us; the launch traced here: 68.2 us
  Pallas kernels  62.6 us (91%)
  local copies, waits for them, and re-layouts  4.97 us (7%)
    pallas_call x1, Pallas kernels, fused(): pl.pallas_call(functools.partial(kernel, NF, NT, C), out_shape=(serve, se...  62.6 us
    unnamed x10, local copies, waits for them, and re-layouts  4.97 us

profile of v4, /device:TPU:0, one launch (start us, length us, event | category | flops | bytes accessed | tf_op | source)
XLA Modules:
  0.0 68.2 jit_solution(6650574458167373285)
XLA Ops:
  0.6 62.6 %shard_map.102 = (bf16[1,2048,128]{2,1,0:T(8,128)(2,1)}, bf16[1,2048,128]{2,1,0:T(8,128)(2,1)}, bf16[1,2048,128]{2,1,0:T(8,128)(2,1)}, bf16[224,512]{1,0:T(8,128)(2,1)}) custom-call(bf16[224,512]{1,0:T(8,128)(2,1)} %tokens.1, s32[2,224]{1,0:T(2,128)} %bitcast.3, f32[2,224]{1,0:T(2,128)} %bitcast.4, f32[1,512]{1,0:T(1,128)} %bitcast.5, f32[4,512,128]{2,1,0:T(8,128)} %gm.1, ...), custom_call_target="tpu_custom_call" | custom-call | tf_op jit(solution)/shard_map/pallas_call | solution.py:482
  63.2 0.0 copy-start.1
  63.2 1.9 %copy.15 = bf16[1,2048,128]{2,1,0:T(8,128)(2,1)} copy(bf16[1,2048,128]{2,1,0:T(8,128)(2,1)} %get-tuple-element.8) | data formatting | bytes 1048576
  65.2 0.0 copy-done.1
  65.2 0.0 copy-start
  65.2 0.8 %copy.16 = bf16[1,2048,128]{2,1,0:T(8,128)(2,1)} copy(bf16[1,2048,128]{2,1,0:T(8,128)(2,1)S(1)} %copy-done.1) | data formatting | bytes 1048576
  65.9 0.4 copy-done
  66.4 0.0 copy-start.2
  66.4 0.8 %copy.17 = bf16[1,2048,128]{2,1,0:T(8,128)(2,1)} copy(bf16[1,2048,128]{2,1,0:T(8,128)(2,1)S(1)} %copy-done) | data formatting | bytes 1048576
  67.2 0.3 copy-done.2
  67.5 0.7 %copy.18 = bf16[224,512]{1,0:T(8,128)(2,1)} copy(bf16[224,512]{1,0:T(8,128)(2,1)S(1)} %copy-done.2) | data formatting | bytes 458752
Async XLA Ops:
  63.2 1.9 %copy-start.1 = (bf16[1,2048,128]{2,1,0:T(8,128)(2,1)S(1)}, bf16[1,2048,128]{2,1,0:T(8,128)(2,1)}, u32[]{:S(2)}) copy-start(bf16[1,2048,128]{2,1,0:T(8,128)(2,1)} %get-tuple-element.9) | copy-start | bytes 1572868
  65.2 1.2 %copy-start = (bf16[1,2048,128]{2,1,0:T(8,128)(2,1)S(1)}, bf16[1,2048,128]{2,1,0:T(8,128)(2,1)}, u32[]{:S(2)}) copy-start(bf16[1,2048,128]{2,1,0:T(8,128)(2,1)} %get-tuple-element.10) | copy-start | bytes 1572868
  66.4 1.1 %copy-start.2 = (bf16[224,512]{1,0:T(8,128)(2,1)S(1)}, bf16[224,512]{1,0:T(8,128)(2,1)}, u32[]{:S(2)}) copy-start(bf16[224,512]{1,0:T(8,128)(2,1)} %get-tuple-element.11) | copy-start | bytes 688132

commit v5 on v4

--- a/solution.py
+++ b/solution.py
@@ -466,6 +466,28 @@
                 hop(tokens, s, p, -1).wait_send()
 
 
+def finish(n, pieces, *refs):
+    ins, outs, stage, sems = refs[:n], refs[n : 2 * n], refs[2 * n : 3 * n], refs[3 * n]
+    cuts = []
+    for i, ref in enumerate(ins):
+        size = ref.shape[-2] // pieces
+        for p in range(pieces):
+            at = (0,) * (len(ref.shape) - 2) + (pl.ds(p * size, size), slice(None))
+            cuts.append((i, p, at))
+    there = {}
+    for i, p, at in cuts:
+        there[i, p] = pltpu.make_async_copy(ins[i].at[at], stage[i].at[at], sems.at[0, i, p])
+        there[i, p].start()
+    back = []
+    for i, p, at in cuts:
+        there[i, p].wait()
+        cp = pltpu.make_async_copy(stage[i].at[at], outs[i].at[at], sems.at[1, i, p])
+        cp.start()
+        back.append(cp)
+    for cp in back:
+        cp.wait()
+
+
 def fused(tokens, route_ids, route_weights, norm_gain, gate_master, up_master, down_master):
     NF, NT = lax.axis_size("fs"), lax.axis_size("tp")
     E, Dl, Fl = gate_master.shape
@@ -479,7 +501,7 @@
     dma = pltpu.SemaphoreType.DMA
     vmem, hbm = pl.BlockSpec(memory_space=pltpu.VMEM), pl.BlockSpec(memory_space=pl.ANY)
     serve = jax.ShapeDtypeStruct((1, D, Fl), bf16)
-    return pl.pallas_call(
+    done = pl.pallas_call(
         functools.partial(kernel, NF, NT, C),
         out_shape=(serve, serve, serve, jax.ShapeDtypeStruct((T, Dq), bf16)),
         in_specs=[vmem] * 4 + [hbm] * 3,
@@ -521,6 +543,15 @@
         tokens, route_ids.T, route_weights.T, norm_gain[None, :],
         gate_master, up_master, down_master,
     )
+    pieces = 2 if T % 32 == 0 else 1
+    return pl.pallas_call(
+        functools.partial(finish, len(done), pieces),
+        out_shape=tuple(jax.ShapeDtypeStruct(a.shape, a.dtype) for a in done),
+        in_specs=[hbm] * len(done),
+        out_specs=(hbm,) * len(done),
+        scratch_shapes=[pltpu.VMEM(a.shape, a.dtype) for a in done] + [dma((2, len(done), pieces))],
+        compiler_params=pltpu.CompilerParams(vmem_limit_bytes=56 * 1024 * 1024),
+    )(*done)
 
 
 def solution(mesh):

time: 69 us -> 66.2 us (0.959)
  local copies, waits for them, and re-layouts: 4.97 us -> 0 us
  Pallas kernels: 62.6 us -> 64.9 us
    unnamed x10 -> x0, local copies, waits for them, and re-layouts: 4.97 us -> none
    pallas_call x0 -> x1, Pallas kernels: none -> 2.29 us  [fused(): pl.pallas_call(functools.partial(finish, len(done), pieces), out_shape=tu...]
where the time goes in v5:
time: 66.2 us; the launch traced here: 65.5 us
  Pallas kernels  64.9 us (98%)
    pallas_call x1, Pallas kernels, fused(): pl.pallas_call(functools.partial(kernel, NF, NT, C), out_shape=(serve, se...  62.6 us
    pallas_call x1, Pallas kernels, fused(): pl.pallas_call(functools.partial(finish, len(done), pieces), out_shape=tu...  2.29 us

profile of v5, /device:TPU:0, one launch (start us, length us, event | category | flops | bytes accessed | tf_op | source)
XLA Modules:
  0.0 65.5 jit_solution(6893871566327364936)
XLA Ops:
  0.6 62.6 %shard_map.102 = (bf16[1,2048,128]{2,1,0:T(8,128)(2,1)}, bf16[1,2048,128]{2,1,0:T(8,128)(2,1)}, bf16[1,2048,128]{2,1,0:T(8,128)(2,1)}, bf16[224,512]{1,0:T(8,128)(2,1)}) custom-call(bf16[224,512]{1,0:T(8,128)(2,1)} %tokens.1, s32[2,224]{1,0:T(2,128)} %bitcast.3, f32[2,224]{1,0:T(2,128)} %bitcast.4, f32[1,512]{1,0:T(1,128)} %bitcast.5, f32[4,512,128]{2,1,0:T(8,128)} %gm.1, ...), custom_call_target="tpu_custom_call" | custom-call | tf_op jit(solution)/shard_map/pallas_call | solution.py:504
  63.2 2.3 %shard_map.103 = (bf16[1,2048,128]{2,1,0:T(8,128)(2,1)}, bf16[1,2048,128]{2,1,0:T(8,128)(2,1)}, bf16[1,2048,128]{2,1,0:T(8,128)(2,1)}, bf16[224,512]{1,0:T(8,128)(2,1)}) custom-call(bf16[1,2048,128]{2,1,0:T(8,128)(2,1)} %get-tuple-element.8.refs_0_, bf16[1,2048,128]{2,1,0:T(8,128)(2,1)} %get-tuple-element.9.refs_1_, ...), custom_call_target="tpu_custom_call" | custom-call | tf_op jit(solution)/shard_map/pallas_call | solution.py:547

commit v6 on v5

--- a/solution.py
+++ b/solution.py
@@ -385,8 +385,9 @@
     for s in near:
         from_peer(wgu, guy_recv, s)
         partial_sums(s, False)
-        to_peer(wd, wdy_send, wdy_recv, wd_recv, s)
-        turn(s, g)
+        if s is not near[-1]:
+            to_peer(wd, wdy_send, wdy_recv, wd_recv, s)
+            turn(s, g)
     outs = [
         pltpu.make_async_copy(wgu.at[:, :Fl], gate_o.at[0], o_sem.at[0]),
         pltpu.make_async_copy(wgu.at[:, Fl:], up_o.at[0], o_sem.at[1]),
@@ -402,6 +403,8 @@
         hid[t, s] = (gate / (1.0 + jnp.exp(-gate)) * up).astype(bf16)
         spread(hid, h_sib, h_x, h_recv, s)
 
+    to_peer(wd, wdy_send, wdy_recv, wd_recv, near[-1])
+    turn(near[-1], g)
     for s in near:
         from_peer(wd, wdy_recv, s)
         turn(s, 1 - g)

time: 66.2 us -> 66.3 us (level)
  no operation moved by 1% of the time
where the time goes in v6:
time: 66.3 us; the launch traced here: 65.6 us
  Pallas kernels  64.9 us (98%)
    pallas_call x1, Pallas kernels, fused(): pl.pallas_call(functools.partial(kernel, NF, NT, C), out_shape=(serve, se...  62.6 us
    pallas_call x1, Pallas kernels, fused(): pl.pallas_call(functools.partial(finish, len(done), pieces), out_shape=tu...  2.29 us

profile of v6, /device:TPU:0, one launch (start us, length us, event | category | flops | bytes accessed | tf_op | source)
XLA Modules:
  0.0 65.6 jit_solution(2093031956311776978)
XLA Ops:
  0.6 62.6 %shard_map.102 = (bf16[1,2048,128]{2,1,0:T(8,128)(2,1)}, bf16[1,2048,128]{2,1,0:T(8,128)(2,1)}, bf16[1,2048,128]{2,1,0:T(8,128)(2,1)}, bf16[224,512]{1,0:T(8,128)(2,1)}) custom-call(bf16[224,512]{1,0:T(8,128)(2,1)} %tokens.1, s32[2,224]{1,0:T(2,128)} %bitcast.3, f32[2,224]{1,0:T(2,128)} %bitcast.4, f32[1,512]{1,0:T(1,128)} %bitcast.5, f32[4,512,128]{2,1,0:T(8,128)} %gm.1, ...), custom_call_target="tpu_custom_call" | custom-call | tf_op jit(solution)/shard_map/pallas_call | solution.py:507
  63.3 2.3 %shard_map.103 = (bf16[1,2048,128]{2,1,0:T(8,128)(2,1)}, bf16[1,2048,128]{2,1,0:T(8,128)(2,1)}, bf16[1,2048,128]{2,1,0:T(8,128)(2,1)}, bf16[224,512]{1,0:T(8,128)(2,1)}) custom-call(bf16[1,2048,128]{2,1,0:T(8,128)(2,1)} %get-tuple-element.8.refs_0_, bf16[1,2048,128]{2,1,0:T(8,128)(2,1)} %get-tuple-element.9.refs_1_, ...), custom_call_target="tpu_custom_call" | custom-call | tf_op jit(solution)/shard_map/pallas_call | solution.py:550
